TPU v7x, 512 devices: a whole 4x4x16 slice. The times are simulated.
512 devices in a mesh: ep: 32 (over z, core), tp: 16 (over y, x).
Axes of the slice: x: 4, y: 4, z: 16, core: 2. Of those that a mesh axis runs over, the one named last changes fastest.
Arguments:
- query_rows: bfloat16 [16384, 2048], P('ep', 'tp'), may hold values from -6 to 6
- key_rows: bfloat16 [16384, 2048], P('ep', 'tp'), may hold values from -6 to 6
- value_rows: bfloat16 [16384, 4096], P('ep', 'tp'), may hold values from -6 to 6
- in_gate: float32 [16, 16384], P('tp', 'ep'), may hold values from -120 to 120
- forget_gate: float32 [16, 16384], P('tp', 'ep'), may hold values from -2 to 20
- out_gate: bfloat16 [16384, 4096], P('ep', 'tp'), may hold values from -6 to 6
- head_gain: float32 [4096], P('tp'), may hold values from 0.1 to 1.9
- mix_weight: bfloat16 [4096, 4096], P(None, 'tp'), may hold values from -0.09375 to 0.09375
- expert_input: bfloat16 [8192, 4096], P('ep', 'tp'), may hold values from -30 to 30
- routes: int32 [8192, 2], P('ep'), may hold values from 0 to 31, all different within a row; in each aligned block of 256 rows (0 to 255, 256 to 511, ...) at most 32 rows name the same one
- route_weight: float32 [8192, 2], P('ep'), may hold values from 0.25 to 1.25
- gate_weight: bfloat16 [32, 1024, 4096], P('ep', 'tp'), may hold values from -0.09375 to 0.09375
- up_weight: bfloat16 [32, 1024, 4096], P('ep', 'tp'), may hold values from -0.09375 to 0.09375
- down_weight: bfloat16 [32, 1024, 4096], P('ep', None, 'tp'), may hold values from -0.1875 to 0.1875
Outputs:
- mixer_out: bfloat16 [16384, 4096], P('ep', 'tp')
- expert_out: bfloat16 [8192, 4096], P('ep', 'tp')
Inputs may be any that keep to these rules, and one draw needn't show every extreme that they name: `routes`: each row names 2 different experts. In the rows of one device no expert is named by more than 32 rows, and in the rows of some device an expert is named by exactly 32 rows.
All inputs are finite; a program needn't handle non-finite values.
Results may differ from a plain program's by a relative error of at most 0.0057.
Values may be sent and summed in bfloat16 or wider, within the bound.
No kernel may reach another device: no remote copies, remote signals or barrier semaphores. Data moves between devices by JAX's collectives and lax.ppermute only.
A program may use at most 128 MiB of HBM per device.

v0:
```python
import jax
import jax.numpy as jnp
from jax import lax
from jax.sharding import Mesh
from jax.sharding import PartitionSpec as P

D = 4096
BLOCK = 64
EP = ("ep_0", "ep_1")
EPSILON = 1e-06
LOG_FLOOR = -1e30
HIGHEST_PRECISION = lax.Precision.HIGHEST


def nothing_yet(x, identity):
    return jax.tree.map(
        lambda part, zero: jnp.zeros_like(part) + jnp.asarray(zero, part.dtype), x, identity
    )


def collected_together(x, axis):
    leaves = jax.tree.leaves(x)
    turns = sorted(range(len(leaves)), key=lambda k: -leaves[k].size)
    width = (1, *leaves[turns[0]].shape)[-1]
    lines = [
        jnp.pad(leaves[k].reshape(-1), (0, -leaves[k].size % width)).reshape(-1, width)
        for k in turns
    ]
    both, at, found = (lax.all_gather(jnp.concatenate(lines), axis), 0, {})
    for k, line in zip(turns, lines):
        share = both[:, at : at + len(line)].reshape(len(both), -1)
        found[k] = share[:, : leaves[k].size].reshape(-1, *leaves[k].shape)
        at += len(line)
    numbers = iter(range(len(leaves)))
    return jax.tree.map(lambda _: found[next(numbers)], x)


def prefix_by_axis(x, axes, combine, identity):
    before = start = nothing_yet(x, identity)
    subtotal = x
    for axis in reversed(axes):
        length, index = (lax.axis_size(axis), lax.axis_index(axis))
        pieces = collected_together(subtotal, axis)
        inside, subtotal = (start, start)
        for k in range(length):
            passed = k < index
            subtotal = combine(subtotal, jax.tree.map(lambda part: part[k], pieces))
            inside = jax.tree.map(lambda new, old: jnp.where(passed, new, old), subtotal, inside)
        before = combine(inside, before)
    return before


def joined_along(tiles, dim):
    dims = list(tiles.shape[1:])
    dims[dim] *= tiles.shape[0]
    return jnp.moveaxis(tiles, 0, dim).reshape(dims)


def copy_for_each(x, axis):
    copies = jnp.broadcast_to(x, (lax.axis_size(axis), *x.shape))
    return lax.all_to_all(copies, axis, split_axis=0, concat_axis=0, tiled=True)


def gather_directly(x, axis, dim):
    return joined_along(copy_for_each(x, axis), dim)


def combine(first_part, second_part):
    decay_first, max_first, memory_first, normal_first = first_part
    decay_second, max_second, memory_second, normal_second = second_part
    running_max = jnp.maximum(decay_second + max_first, max_second)
    keep_first = jnp.exp(decay_second + max_first - running_max)
    keep_second = jnp.exp(max_second - running_max)
    memory = (
        keep_first[..., None, None] * memory_first + keep_second[..., None, None] * memory_second
    )
    normalizer = keep_first[..., None] * normal_first + keep_second[..., None] * normal_second
    return (decay_first + decay_second, running_max, memory, normalizer)


def identity_state(head_count, key_width, value_width):
    return (
        jnp.zeros((head_count,), jnp.float32),
        jnp.full((head_count,), LOG_FLOOR, jnp.float32),
        jnp.zeros((head_count, key_width, value_width), jnp.float32),
        jnp.zeros((head_count, key_width), jnp.float32),
    )


def halfprod(form, left, right):
    return jnp.einsum(form, left, right, preferred_element_type=jnp.float32)


def prepare(query_heads, key_heads, value_heads, in_gate, forget_gate):
    head_count, length, key_width = query_heads.shape
    block_count = length // BLOCK
    query_blocks = query_heads.reshape(head_count, block_count, BLOCK, key_width)
    key_blocks = key_heads.reshape(head_count, block_count, BLOCK, key_width)
    value_blocks = value_heads.reshape(head_count, block_count, BLOCK, value_heads.shape[-1])
    log_input = in_gate.reshape(head_count, block_count, BLOCK)
    cumulative = jnp.cumsum(
        jax.nn.log_sigmoid(forget_gate).reshape(head_count, block_count, BLOCK), axis=-1
    )
    block_decay = cumulative[..., -1]
    weight_log = block_decay[..., None] - cumulative + log_input
    block_max = jnp.max(weight_log, axis=-1)
    weighted = (
        key_blocks.astype(jnp.float32) * jnp.exp(weight_log - block_max[..., None])[..., None]
    )
    normalizer = jnp.sum(weighted, axis=2)
    memory = halfprod("hcsk,hcsv->hckv", weighted.astype(jnp.bfloat16), value_blocks)
    return (
        (query_blocks, key_blocks, value_blocks, log_input, cumulative),
        (block_decay, block_max, memory, normalizer),
    )


def prefix(summary, initial):
    leading = jax.tree.map(lambda tensor: jnp.moveaxis(tensor, 1, 0), summary)

    def advance(running, current):
        return (combine(running, current), running)

    final_state, before = lax.scan(advance, initial, leading)
    return (final_state, jax.tree.map(lambda tensor: jnp.moveaxis(tensor, 0, 1), before))


def block_outputs(blocked, before):
    query_blocks, key_blocks, value_blocks, log_input, cumulative = blocked
    prior_max, prior_memory, prior_normal = (before[1], before[2], before[3])
    block_len = cumulative.shape[-1]
    scale = query_blocks.shape[-1] ** (-0.5)
    causal = jnp.tril(jnp.ones((block_len, block_len), dtype=bool))
    log_decay = jnp.where(
        causal,
        cumulative[..., :, None] - cumulative[..., None, :] + log_input[..., None, :],
        -jnp.inf,
    )
    log_inter = cumulative + prior_max[..., None]
    top_value = jnp.maximum(log_inter, jnp.max(log_decay, axis=-1))
    scores = (
        halfprod("hctk,hcsk->hcts", query_blocks, key_blocks)
        * scale
        * jnp.exp(log_decay - top_value[..., None])
    )
    carried = jnp.exp(log_inter - top_value) * scale
    query_wide = query_blocks.astype(jnp.float32)
    numerator = carried[..., None] * jnp.einsum(
        "hctk,hckv->hctv", query_wide, prior_memory, precision=HIGHEST_PRECISION
    ) + halfprod("hcts,hcsv->hctv", scores.astype(jnp.bfloat16), value_blocks)
    denominator = carried * jnp.einsum(
        "hctk,hck->hct", query_wide, prior_normal, precision=HIGHEST_PRECISION
    ) + jnp.sum(scores, axis=-1)
    return numerator / jnp.maximum(jnp.abs(denominator), jnp.exp(-top_value))[..., None]


def finish(head_values, out_gate, head_gain):
    head_count, block_count, block_len, value_width = head_values.shape
    per_head = jnp.transpose(head_values, (1, 2, 0, 3)).reshape(
        block_count * block_len, head_count, value_width
    )
    per_head = per_head * lax.rsqrt(jnp.mean(per_head * per_head, axis=-1, keepdims=True) + EPSILON)
    per_head = per_head.reshape(block_count * block_len, head_count * value_width) * head_gain
    per_head = per_head * jax.nn.sigmoid(out_gate.astype(jnp.float32))
    return per_head.astype(jnp.bfloat16)


def cell_heads(query_rows, key_rows, value_rows, in_gate, forget_gate, out_gate, head_gain):
    length = query_rows.shape[0]
    head_count = in_gate.shape[0]
    key_width = query_rows.shape[1] // head_count
    value_width = value_rows.shape[1] // head_count
    query_heads = query_rows.reshape(length, head_count, key_width).transpose(1, 0, 2)
    key_heads = key_rows.reshape(length, head_count, key_width).transpose(1, 0, 2)
    value_heads = value_rows.reshape(length, head_count, value_width).transpose(1, 0, 2)
    blocked, summary = prepare(query_heads, key_heads, value_heads, in_gate, forget_gate)
    initial = identity_state(head_count, key_width, value_width)
    final_state, before = prefix(summary, initial)
    incoming = prefix_by_axis(final_state, EP, combine, initial)
    expanded = jax.tree.map(lambda tensor: tensor[:, None], incoming)
    before = combine(expanded, before)
    return finish(block_outputs(blocked, before), out_gate, head_gain)


def body(
    query_rows,
    key_rows,
    value_rows,
    in_gate,
    forget_gate,
    out_gate,
    head_gain,
    mix_weight,
    expert_input,
    routes,
    route_weight,
    gate_weight,
    up_weight,
    down_weight,
):
    mixed_heads = cell_heads(
        query_rows, key_rows, value_rows, in_gate, forget_gate, out_gate, head_gain
    )
    gate_local = gate_weight[0]
    up_local = up_weight[0]
    down_local = down_weight[0]
    group_size = lax.axis_size(EP)
    token_count, fanout = routes.shape
    capacity = 2 * token_count * fanout // group_size
    slot_count = group_size * capacity
    chosen = routes.reshape(-1)
    one_hot = (chosen[:, None] == jnp.arange(group_size, dtype=jnp.int32)[None, :]).astype(
        jnp.int32
    )
    position = jnp.sum((jnp.cumsum(one_hot, axis=0) - one_hot) * one_hot, axis=1)
    target = chosen * capacity + position
    matches = (jnp.arange(slot_count, dtype=jnp.int32)[:, None] == target[None, :]).astype(
        jnp.int32
    )
    occupied = jnp.sum(matches, axis=1) > 0
    source_row = jnp.sum(
        matches * (jnp.arange(token_count * fanout, dtype=jnp.int32) // fanout)[None, :], axis=1
    )
    arrived = lax.all_to_all(
        jnp.where(
            occupied[:, None],
            jnp.take(expert_input, source_row, axis=0),
            jnp.zeros((), expert_input.dtype),
        ),
        EP,
        split_axis=0,
        concat_axis=0,
        tiled=True,
    )
    head_piece = lax.all_gather(mixed_heads, "tp", axis=1, tiled=True)
    token_piece = lax.all_gather(arrived, "tp", axis=1, tiled=True)
    mix_acc = jnp.dot(head_piece, mix_weight, preferred_element_type=jnp.float32)
    gate_acc = jnp.einsum("sd,fd->sf", token_piece, gate_local, preferred_element_type=jnp.float32)
    up_acc = jnp.einsum("sd,fd->sf", token_piece, up_local, preferred_element_type=jnp.float32)
    squares = jnp.sum(jnp.square(token_piece.astype(jnp.float32)), axis=1)
    mix_acc, gate_acc, up_acc, squares = (mix_acc, gate_acc, up_acc, squares)
    mixer_out = mix_acc.astype(jnp.bfloat16)
    inverse_rms = lax.rsqrt(squares / D + EPSILON)[:, None]
    hidden = (jax.nn.silu(gate_acc * inverse_rms) * (up_acc * inverse_rms)).astype(jnp.bfloat16)
    expert_rows = jnp.dot(
        gather_directly(hidden, "tp", 1), down_local, preferred_element_type=jnp.float32
    )
    returned_rows = lax.all_to_all(
        expert_rows.astype(jnp.bfloat16), EP, split_axis=0, concat_axis=0, tiled=True
    )
    picked_rows = (
        jnp.take(returned_rows, target, axis=0).reshape(token_count, fanout, -1).astype(jnp.float32)
    )
    expert_out = jnp.sum(picked_rows * route_weight[:, :, None], axis=1).astype(jnp.bfloat16)
    return (mixer_out, expert_out)


def solution(mesh):
    split = Mesh(mesh.devices.reshape(16, 2, mesh.shape["tp"]), ("ep_0", "ep_1", "tp"))
    in_specs = (
        P(EP, "tp"),
        P(EP, "tp"),
        P(EP, "tp"),
        P("tp", EP),
        P("tp", EP),
        P(EP, "tp"),
        P("tp"),
        P(None, "tp"),
        P(EP, "tp"),
        P(EP, None),
        P(EP, None),
        P(EP, "tp", None),
        P(EP, "tp", None),
        P(EP, None, "tp"),
    )
    out_specs = (P(EP, "tp"), P(EP, "tp"))
    return jax.shard_map(body, mesh=split, in_specs=in_specs, out_specs=out_specs, check_vma=False)
```

profile of v0, /device:TPU:1, one launch (start us, length us, event | category | flops | bytes accessed | tf_op | source)
XLA Modules:
  0.0 352.5 jit_solution(5622983685871281707)
XLA Ops:
  7.3 0.8 fusion.55
  9.1 1.3 reduce.22
  10.6 0.8 reshape.1181
  11.6 1.1 fusion.21
  12.6 1.5 convolution_bitcast_fusion
  14.2 36.5 %while.25 = (s32[]{:T(128)}, f32[1]{0:T(128)}, f32[1]{0:T(128)}, f32[1,128,256]{2,1,0:T(8,128)S(1)}, f32[1,128]{1,0:T(1,128)S(1)}, /*index=5*/f32[8,1]{0,1:T(1,1...) while((s32[]{:T(128)}, f32[1]{0:T(128)}, f32[1]{0:T(128)}, ...), condition=%wide.region_4.5_spmd.clone, body=%wide.region_3.4_spmd.clone.sunk | while | flops 164488 | bytes 659258 | solution.py:124
  25.7 0.7 bitcast_dynamic-update-slice_fusion.2
  30.3 0.7 bitcast_dynamic-update-slice_fusion.2
  34.9 0.7 bitcast_dynamic-update-slice_fusion.2
  51.2 8.5 %all-gather.2 = f32[2,131,256]{2,1,0:T(8,128)S(1)} all-gather(f32[1,131,256]{2,1,0:T(8,128)S(1)} %maximum_bitcast_fusion), channel_id=2, replica_groups=mesh['ep_0'=16,'ep_1'=2,'tp'=16] {'ep_1'}, dimensions={0}, use_global_device_ids=true | all-gather | bytes 402432 | tf_op jit(solution)/shard_map/all_gather | solution.py:29
  66.3 0.7 maximum_bitcast_fusion.1
  67.0 0.8 copy.54
  68.1 1.2 reduce-window.6
  70.5 3.9 %gather_fusion = bf16[1024,256]{1,0:T(8,128)(2,1)S(1)} fusion(bf16[256,256]{1,0:T(8,128)(2,1)S(1)} %copy-done.1, s32[1024]{0:T(1024)S(1)} %broadcast_clamp_fusion), kind=kCustom, calls=%fused_computation | custom fusion | bytes 1052672 | tf_op jit(solution)/shard_map/jit(_take)/gather | solution.py:227
  74.9 48.4 %all_to_all.26 = bf16[32,32,256]{2,1,0:T(8,128)(2,1)} all-to-all(bf16[32,32,256]{2,1,0:T(8,128)(2,1)S(1)} %select_select_fusion), channel_id=1, replica_groups=mesh['ep_0'=16,'ep_1'=2,'tp'=16] {'ep_0','ep_1'}, dimensions={0} | all-to-all | bytes 1048576 | tf_op jit(solution)/shard_map/all_to_all | solution.py:224
  124.7 22.1 %all-gather.12.cloned.1.call-done = f32[16,131,256]{2,1,0:T(8,128)} async-done(((f32[1,131,256]{2,1,0:T(8,128)}), f32[16,131,256]{2,1,0:T(8,128)}) %all-gather.12.cloned.1.call-update) | async-done | bytes 2146320 | tf_op jit(solution)/shard_map/all_gather | solution.py:29
  146.8 1.1 fusion.82
  181.0 2.0 fusion.26
  183.3 0.8 multiply_reduce_fusion.2
  184.2 0.9 fusion.17
  185.1 59.3 %all-gather.10.cloned.1.call-done = bf16[1024,4096]{1,0:T(8,128)(2,1)} async-done(((bf16[1024,256]{1,0:T(8,128)(2,1)}), bf16[1024,4096]{1,0:T(8,128)(2,1)}) %all-gather.10.cloned.1.call-update) | async-done | bytes 8388624 | tf_op jit(solution)/shard_map/all_gather | solution.py:236
  244.4 5.2 %multiply_reduce_fusion = f32[1024]{0:T(1024)S(1)} fusion(bf16[1024,4096]{1,0:T(8,128)(2,1)} %all-gather.10.cloned.1.call-done), kind=kLoop, calls=%fused_computation.12 | loop fusion | flops 12581888 | bytes 8392704 | tf_op jit(solution)/shard_map/reduce_sum | solution.py:240
  250.1 2.7 convolution_multiply_fusion.3
  252.8 2.7 fusion.8
  255.8 35.5 %all_to_all.27 = bf16[16,1024,64]{1,2,0:T(8,128)(2,1)S(1)} all-to-all(bf16[16,1024,64]{1,2,0:T(8,128)(2,1)S(1)} %broadcast_in_dim.75), channel_id=1, replica_groups=mesh['ep_0'=16,'ep_1'=2,'tp'=16] {'tp'}, dimensions={0} | all-to-all | bytes 4194304 | tf_op jit(solution)/shard_map/all_to_all | solution.py:61
  291.3 1.6 convolution_convert_fusion
  292.9 15.3 %all-to-all-start.2 = ((bf16[32,32,256]{2,1,0:T(8,128)(2,1)}), bf16[32,32,256]{2,1,0:T(8,128)(2,1)S(1)}, u32[]{:S(2)}, u32[]{:S(2)}) async-start(bf16[32,32,256]{2,1,0:T(8,128)(2,1)} %bitcast.139), calls=%async_computation.2 | async-start | bytes 1048576 | tf_op jit(solution)/shard_map/all_to_all | solution.py:248
  309.1 22.7 %all-gather.8.cloned.1.call-done = bf16[512,4096]{1,0:T(8,128)(2,1)} async-done(((bf16[512,256]{1,0:T(8,128)(2,1)}), bf16[512,4096]{1,0:T(8,128)(2,1)}) %all-gather.8.cloned.1.call-update) | async-done | bytes 4194320 | tf_op jit(solution)/shard_map/all_gather | solution.py:235
  331.8 4.1 %convolution_convert_fusion.1 = bf16[512,256]{1,0:T(8,128)(2,1)} fusion(bf16[512,4096]{1,0:T(8,128)(2,1)} %all-gather.8.cloned.1.call-done, bf16[4096,256]{1,0:T(8,128)(2,1)S(1)} %copy-done), kind=kOutput, calls=%fused_computation.22 | convolution fusion | flops 1073872896 | bytes 6553600 | tf_op jit(solution)/shard_map/dot_general | solution.py:237
  335.9 5.8 %all-to-all-done.2 = bf16[32,32,256]{2,1,0:T(8,128)(2,1)S(1)} async-done(((bf16[32,32,256]{2,1,0:T(8,128)(2,1)}), bf16[32,32,256]{2,1,0:T(8,128)(2,1)S(1)}, u32[]{:S(2)}, u32[]{:S(2)}) %all-to-all-start.2) | async-done | bytes 524320 | tf_op jit(solution)/shard_map/all_to_all | solution.py:248
  341.7 1.9 gather_fusion.1
  343.8 2.2 multiply_reduce_fusion.1
  (182 shorter events, 24.8 us)
Async XLA Ops:
  7.2 324.6 %copy-start = (bf16[4096,256]{1,0:T(8,128)(2,1)S(1)}, bf16[4096,256]{1,0:T(8,128)(2,1)}, u32[]{:S(2)}) copy-start(bf16[4096,256]{1,0:T(8,128)(2,1)} %param.23) | copy-start | bytes 6291460
  7.2 139.6 %all-gather.12.cloned.1.call-start = ((), (), s32[]{:S(2)}) async-start(), calls=%async_computation.5 | async-start | bytes 2367488 | tf_op jit(solution)/shard_map/all_gather | solution.py:29
  8.4 5.7 %copy-start.7 = (f32[1,8,64]{2,1,0:T(8,128)}, f32[1,8,64]{2,1,0:T(8,128)S(1)}, u32[]{:S(2)}) copy-start(f32[1,8,64]{2,1,0:T(8,128)S(1)} %reduce_window_sum.28) | copy-start | bytes 6148
  11.3 2.8 copy-start.9
  14.1 56.4 %copy-start.1 = (bf16[256,256]{1,0:T(8,128)(2,1)S(1)}, bf16[256,256]{1,0:T(8,128)(2,1)}, u32[]{:S(2)}) copy-start(bf16[256,256]{1,0:T(8,128)(2,1)} %param.24) | copy-start | bytes 393220
  50.6 0.5 copy-start.15
  50.6 0.6 copy-start.17
  67.0 177.4 %all-gather.10.cloned.1.call-start = ((), (), s32[]{:S(2)}) async-start(), calls=%async_computation.4 | async-start | bytes 8912896 | tf_op jit(solution)/shard_map/all_gather | solution.py:236
  74.5 49.9 %copy-start.8 = (f32[1,8,64]{2,1,0:T(8,128)S(1)}, f32[1,8,64]{2,1,0:T(8,128)}, u32[]{:S(2)}) copy-start(f32[1,8,64]{2,1,0:T(8,128)} %copy-done.7) | copy-start | bytes 6148
  74.5 49.9 %copy-start.10 = (f32[8,64]{1,0:T(8,128)S(1)}, f32[8,64]{1,0:T(8,128)}, u32[]{:S(2)}) copy-start(f32[8,64]{1,0:T(8,128)} %copy-done.9) | copy-start | bytes 6148
  74.5 105.5 %copy-start.16 = (f32[8,1]{0,1:T(1,128)S(1)}, f32[8,1]{0,1:T(1,128)}, u32[]{:S(2)}) copy-start(f32[8,1]{0,1:T(1,128)} %copy-done.15) | copy-start | bytes 100
  74.5 105.5 %copy-start.18 = (f32[8,1]{0,1:T(1,128)S(1)}, f32[8,1]{0,1:T(1,128)}, u32[]{:S(2)}) copy-start(f32[8,1]{0,1:T(1,128)} %copy-done.17) | copy-start | bytes 100
  74.5 105.7 %copy-start.12 = (f32[8,1,128]{2,1,0:T(1,128)S(1)}, f32[8,1,128]{2,1,0:T(1,128)}, u32[]{:S(2)}) copy-start(f32[8,1,128]{2,1,0:T(1,128)} %get-tuple-element.83) | copy-start | bytes 12292
  74.5 105.8 %copy-start.22 = (bf16[512,128]{1,0:T(8,128)(2,1)S(1)}, bf16[512,128]{1,0:T(8,128)(2,1)}, u32[]{:S(2)}) copy-start(bf16[512,128]{1,0:T(8,128)(2,1)} %param.16) | copy-start | bytes 393220
  74.5 106.1 %copy-start.5 = (bf16[512,128]{1,0:T(8,128)(2,1)S(1)}, bf16[512,128]{1,0:T(8,128)(2,1)}, u32[]{:S(2)}) copy-start(bf16[512,128]{1,0:T(8,128)(2,1)} %param.17) | copy-start | bytes 393220
  123.3 59.7 %copy-start.3 = (bf16[512,256]{1,0:T(8,128)(2,1)S(1)}, bf16[512,256]{1,0:T(8,128)(2,1)}, u32[]{:S(2)}) copy-start(bf16[512,256]{1,0:T(8,128)(2,1)} %param.18) | copy-start | bytes 786436
  123.3 208.4 %all-gather.8.cloned.1.call-start = ((), (), s32[]{:S(2)}) async-start(), calls=%async_computation.3 | async-start | bytes 4456448 | tf_op jit(solution)/shard_map/all_gather | solution.py:235
  180.3 3.0 copy-start.19
  180.3 3.0 copy-start.23
  183.0 1.2 copy-start.6
  183.0 1.2 copy-start.14
  184.2 65.4 %copy-start.4 = (bf16[1,64,4096]{2,1,0:T(8,128)(2,1)S(1)}, bf16[1,64,4096]{2,1,0:T(8,128)(2,1)}, u32[]{:S(2)}) copy-start(bf16[1,64,4096]{2,1,0:T(8,128)(2,1)} %param.27) | copy-start | bytes 1572868
  244.4 5.8 %copy-start.2 = (bf16[1024,4096]{1,0:T(8,128)(2,1)S(1)}, bf16[1024,4096]{1,0:T(8,128)(2,1)}, u32[]{:S(2)}) copy-start(bf16[1024,4096]{1,0:T(8,128)(2,1)} %all-gather.10.cloned.1.call-done) | copy-start | bytes 25165828
  250.1 2.7 copy-start.20
  255.8 35.5 %copy-start.21 = (bf16[1,1024,256]{2,1,0:T(8,128)(2,1)S(1)}, bf16[1,1024,256]{2,1,0:T(8,128)(2,1)}, u32[]{:S(2)}) copy-start(bf16[1,1024,256]{2,1,0:T(8,128)(2,1)} %param.29) | copy-start | bytes 1572868
  291.3 17.0 %copy-start.11 = (s32[256,2]{0,1:T(2,128)S(1)}, s32[256,2]{0,1:T(2,128)}, u32[]{:S(2)}) copy-start(s32[256,2]{0,1:T(2,128)} %param.25) | copy-start | bytes 6148
  291.3 17.6 %copy-start.13 = (f32[256,2]{0,1:T(2,128)S(1)}, f32[256,2]{0,1:T(2,128)}, u32[]{:S(2)}) copy-start(f32[256,2]{0,1:T(2,128)} %param.26) | copy-start | bytes 6148
  292.9 48.8 %all-to-all-start.2 = ((bf16[32,32,256]{2,1,0:T(8,128)(2,1)}), bf16[32,32,256]{2,1,0:T(8,128)(2,1)S(1)}, u32[]{:S(2)}, u32[]{:S(2)}) async-start(bf16[32,32,256]{2,1,0:T(8,128)(2,1)} %bitcast.139), calls=%async_computation.2 | async-start | bytes 1048576 | tf_op jit(solution)/shard_map/all_to_all | solution.py:248
Sparse Core Ops, SparseCore 0:
  67.1 79.6 all-gather.11
  149.7 94.5 all-gather.9
  247.9 83.7 all-gather.7
where the time goes:
time: 354 us; the launch traced here: 352 us
  waiting for transfers between devices  110 us (31%)
  blocking collectives  92.4 us (26%)
  between operations  51.3 us (14%)
  other arithmetic  28 us (8%)
  local copies, waits for them, and re-layouts  21.5 us (6%)
  loops' own time  19.7 us (6%)
  starting transfers between devices  15.6 us (4%)
  matrix products  14.2 us (4%)
    all_gather x1, waiting for transfers between devices, body(): token_piece = lax.all_gather(arrived, 'tp', axis=1, tiled=True)  59.3 us
    all_to_all x1, blocking collectives, body(): lax.all_to_all(jnp.where(occupied[:, None], jnp.take(expert_input, source...  48.4 us
    all_to_all x1, blocking collectives, copy_for_each(): return lax.all_to_all(copies, axis, split_axis=0, concat_axis=0, tiled=True)  35.5 us
    all_gather x1, waiting for transfers between devices, body(): head_piece = lax.all_gather(mixed_heads, 'tp', axis=1, tiled=True)  22.7 us
    all_gather x1, waiting for transfers between devices, collected_together(): both, at, found = (lax.all_gather(jnp.concatenate(lines), axis), 0, {})  22.1 us
    another operation x1, loops' own time, prefix(): final_state, before = lax.scan(advance, initial, leading)  19.7 us
    all_to_all x1, starting transfers between devices, body(): lax.all_to_all(expert_rows.astype(jnp.bfloat16), EP, split_axis=0, concat...  15.3 us
    dynamic_update_slice x16, other arithmetic, prefix(): final_state, before = lax.scan(advance, initial, leading)  9.85 us
  transfers between devices with their start and end apart: 4, of which 4 were waited for; matrix products, arithmetic and copies ran while one was open for 9% of the time, Pallas kernels for 0%

commit v1 on v0

--- a/solution.py
+++ b/solution.py
@@ -232,7 +232,8 @@
         concat_axis=0,
         tiled=True,
     )
-    head_piece = lax.all_gather(mixed_heads, "tp", axis=1, tiled=True)
+    repeated = jnp.stack([mixed_heads] * lax.axis_size("tp"))
+    head_piece = jnp.concatenate(lax.all_to_all(repeated, "tp", 0, 0), axis=1)
     token_piece = lax.all_gather(arrived, "tp", axis=1, tiled=True)
     mix_acc = jnp.dot(head_piece, mix_weight, preferred_element_type=jnp.float32)
     gate_acc = jnp.einsum("sd,fd->sf", token_piece, gate_local, preferred_element_type=jnp.float32)

time: 354 us -> 420 us (1.19)
  waiting for transfers between devices: 110 us -> 192 us
  blocking collectives: 92.4 us -> 57.1 us
  starting transfers between devices: 15.6 us -> 27.8 us
  local copies, waits for them, and re-layouts: 21.5 us -> 25.8 us
    all_to_all x0 -> x2, waiting for transfers between devices: none -> 78 us  [the longest x1 55.9 us: body(): head_piece = jnp.concatenate(lax.all_to_all(repeated, 'tp', 0, 0), axis=1)]
    all_to_all x1 -> x0, blocking collectives: 35.5 us -> none  [copy_for_each(): return lax.all_to_all(copies, axis, split_axis=0, concat_axis=0, tiled=True)]
    all_gather x1 -> x0, waiting for transfers between devices: 22.7 us -> none  [body(): head_piece = lax.all_gather(mixed_heads, 'tp', axis=1, tiled=True)]
    all_to_all x1, waiting for transfers between devices: 5.79 us -> 28.4 us  [body(): lax.all_to_all(expert_rows.astype(jnp.bfloat16), EP, split_axis=0, concat...]
    all_to_all x0 -> x2, starting transfers between devices: none -> 12.3 us  [the longest x1 7.44 us: body(): head_piece = jnp.concatenate(lax.all_to_all(repeated, 'tp', 0, 0), axis=1)]
  transfers between devices with their start and end apart: 4 -> 5, of which waited for: 4 -> 5; matrix products, arithmetic and copies ran while one was open for 9% -> 6% of each run, Pallas kernels for 0% -> 0%
where the time goes in v1:
time: 420 us; the launch traced here: 419 us
  waiting for transfers between devices  192 us (46%)
  blocking collectives  57.1 us (14%)
  between operations  52 us (12%)
  starting transfers between devices  27.8 us (7%)
  other arithmetic  27.1 us (6%)
  local copies, waits for them, and re-layouts  25.8 us (6%)
  loops' own time  20.9 us (5%)
  matrix products  15.8 us (4%)
    all_gather x1, waiting for transfers between devices, body(): token_piece = lax.all_gather(arrived, 'tp', axis=1, tiled=True)  62.8 us
    all_to_all x1, waiting for transfers between devices, body(): head_piece = jnp.concatenate(lax.all_to_all(repeated, 'tp', 0, 0), axis=1)  55.9 us
    all_to_all x1, blocking collectives, body(): lax.all_to_all(jnp.where(occupied[:, None], jnp.take(expert_input, source...  48.6 us
    all_to_all x1, waiting for transfers between devices, body(): lax.all_to_all(expert_rows.astype(jnp.bfloat16), EP, split_axis=0, concat...  28.4 us
    all_gather x1, waiting for transfers between devices, collected_together(): both, at, found = (lax.all_gather(jnp.concatenate(lines), axis), 0, {})  22.8 us
    all_to_all x1, waiting for transfers between devices, copy_for_each(): return lax.all_to_all(copies, axis, split_axis=0, concat_axis=0, tiled=True)  22.1 us
    another operation x1, loops' own time, prefix(): final_state, before = lax.scan(advance, initial, leading)  20.9 us
    all_to_all x1, starting transfers between devices, body(): lax.all_to_all(expert_rows.astype(jnp.bfloat16), EP, split_axis=0, concat...  15.4 us
  transfers between devices with their start and end apart: 5, of which 5 were waited for; matrix products, arithmetic and copies ran while one was open for 6% of the time, Pallas kernels for 0%

profile of v1, /device:TPU:1, one launch (start us, length us, event | category | flops | bytes accessed | tf_op | source)
XLA Modules:
  0.0 418.6 jit_solution(3138331151573554497)
XLA Ops:
  7.3 0.8 fusion.55
  9.1 1.3 reduce.22
  10.6 0.8 reshape.1189
  11.6 1.1 fusion.21
  12.6 1.5 convolution_bitcast_fusion
  14.2 37.9 %while.25 = (s32[]{:T(128)}, f32[1]{0:T(128)}, f32[1]{0:T(128)}, f32[1,128,256]{2,1,0:T(8,128)S(1)}, f32[1,128]{1,0:T(1,128)S(1)}, /*index=5*/f32[8,1]{0,1:T(1,1...) while((s32[]{:T(128)}, f32[1]{0:T(128)}, f32[1]{0:T(128)}, ...), condition=%wide.region_4.5_spmd.clone, body=%wide.region_3.4_spmd.clone.sunk | while | flops 164488 | bytes 659258 | solution.py:124
  50.0 0.7 bitcast_dynamic-update-slice_fusion.2
  52.6 8.5 %all-gather.2 = f32[2,131,256]{2,1,0:T(8,128)S(1)} all-gather(f32[1,131,256]{2,1,0:T(8,128)S(1)} %maximum_bitcast_fusion), channel_id=2, replica_groups=mesh['ep_0'=16,'ep_1'=2,'tp'=16] {'ep_1'}, dimensions={0}, use_global_device_ids=true | all-gather | bytes 402432 | tf_op jit(solution)/shard_map/all_gather | solution.py:29
  68.3 0.8 copy.58
  69.4 1.2 reduce-window.6
  71.8 3.9 gather_fusion
  76.1 48.6 %all_to_all.31 = bf16[32,32,256]{2,1,0:T(8,128)(2,1)} all-to-all(bf16[32,32,256]{2,1,0:T(8,128)(2,1)S(1)} %select_select_fusion), channel_id=1, replica_groups=mesh['ep_0'=16,'ep_1'=2,'tp'=16] {'ep_0','ep_1'}, dimensions={0} | all-to-all | bytes 1048576 | tf_op jit(solution)/shard_map/all_to_all | solution.py:224
  125.9 22.8 %all-gather.9.cloned.1.call-done = f32[16,131,256]{2,1,0:T(8,128)} async-done(((f32[1,131,256]{2,1,0:T(8,128)}), f32[16,131,256]{2,1,0:T(8,128)}) %all-gather.9.cloned.1.call-update) | async-done | bytes 2146320 | tf_op jit(solution)/shard_map/all_gather | solution.py:29
  148.7 1.1 fusion.82
  182.8 62.8 %all-gather.7.cloned.1.call-done = bf16[1024,4096]{1,0:T(8,128)(2,1)} async-done(((bf16[1024,256]{1,0:T(8,128)(2,1)}), bf16[1024,4096]{1,0:T(8,128)(2,1)}) %all-gather.7.cloned.1.call-update) | async-done | bytes 8388624 | tf_op jit(solution)/shard_map/all_gather | solution.py:237
  245.5 5.2 %multiply_reduce_fusion = f32[1024]{0:T(1024)S(1)} fusion(bf16[1024,4096]{1,0:T(8,128)(2,1)} %all-gather.7.cloned.1.call-done), kind=kLoop, calls=%fused_computation.12 | loop fusion | flops 12581888 | bytes 8392704 | tf_op jit(solution)/shard_map/reduce_sum | solution.py:241
  251.3 2.7 convolution_multiply_fusion.3
  254.0 2.7 fusion.8
  256.7 1.6 broadcast_in_dim.75
  258.3 4.9 %all-to-all-start.2 = ((bf16[16,1024,64]{1,2,0:T(8,128)(2,1)}), bf16[16,1024,64]{1,2,0:T(8,128)(2,1)}, u32[]{:S(2)}, u32[]{:S(2)}) async-start(bf16[16,1024,64]{1,2,0:T(8,128)(2,1)} %broadcast_in_dim.75), calls=%async_computation.2 | async-start | bytes 4194304 | tf_op jit(solution)/shard_map/all_to_all | solution.py:61
  263.9 2.0 fusion.26
  266.2 0.8 multiply_reduce_fusion.2
  267.4 22.1 %all-to-all-done.2 = bf16[16,1024,64]{1,2,0:T(8,128)(2,1)} async-done(((bf16[16,1024,64]{1,2,0:T(8,128)(2,1)}), bf16[16,1024,64]{1,2,0:T(8,128)(2,1)}, u32[]{:S(2)}, u32[]{:S(2)}) %all-to-all-start.2) | async-done | bytes 2097184 | tf_op jit(solution)/shard_map/all_to_all | solution.py:61
  289.6 2.5 stack.2
  292.1 7.4 %all-to-all-start = ((bf16[16,512,256]{1,2,0:T(8,128)(2,1)}), bf16[16,512,256]{1,2,0:T(8,128)(2,1)}, u32[]{:S(2)}, u32[]{:S(2)}) async-start(bf16[16,512,256]{1,2,0:T(8,128)(2,1)} %stack.2), calls=%async_computation | async-start | bytes 8388608 | tf_op jit(solution)/shard_map/all_to_all | solution.py:236
  299.6 3.2 convolution_convert_fusion
  302.7 55.9 %all-to-all-done = bf16[16,512,256]{1,2,0:T(8,128)(2,1)} async-done(((bf16[16,512,256]{1,2,0:T(8,128)(2,1)}), bf16[16,512,256]{1,2,0:T(8,128)(2,1)}, u32[]{:S(2)}, u32[]{:S(2)}) %all-to-all-start) | async-done | bytes 4194336 | tf_op jit(solution)/shard_map/all_to_all | solution.py:236
  358.6 15.4 %all-to-all-start.3 = ((bf16[32,32,256]{2,1,0:T(8,128)(2,1)}), bf16[32,32,256]{2,1,0:T(8,128)(2,1)S(1)}, u32[]{:S(2)}, u32[]{:S(2)}) async-start(bf16[32,32,256]{2,1,0:T(8,128)(2,1)} %bitcast.141), calls=%async_computation.3 | async-start | bytes 1048576 | tf_op jit(solution)/shard_map/all_to_all | solution.py:249
  375.0 4.2 %convolution_convert_fusion.1 = bf16[512,256]{1,0:T(8,128)(2,1)} fusion(bf16[512,4096]{0,1:T(8,128)(2,1)} %bitcast.130, bf16[4096,256]{1,0:T(8,128)(2,1)S(1)} %copy-done), kind=kOutput, calls=%fused_computation.22 | convolution fusion | flops 1073872896 | bytes 6553600 | tf_op jit(solution)/shard_map/dot_general | solution.py:238
  379.1 28.4 %all-to-all-done.3 = bf16[32,32,256]{2,1,0:T(8,128)(2,1)S(1)} async-done(((bf16[32,32,256]{2,1,0:T(8,128)(2,1)}), bf16[32,32,256]{2,1,0:T(8,128)(2,1)S(1)}, u32[]{:S(2)}, u32[]{:S(2)}) %all-to-all-start.3) | async-done | bytes 524320 | tf_op jit(solution)/shard_map/all_to_all | solution.py:249
  407.5 1.9 gather_fusion.1
  409.6 2.2 multiply_reduce_fusion.1
  (182 shorter events, 26.8 us)
Async XLA Ops:
  7.2 367.8 %copy-start = (bf16[4096,256]{1,0:T(8,128)(2,1)S(1)}, bf16[4096,256]{1,0:T(8,128)(2,1)}, u32[]{:S(2)}) copy-start(bf16[4096,256]{1,0:T(8,128)(2,1)} %param.23) | copy-start | bytes 6291460
  7.2 141.5 %all-gather.9.cloned.1.call-start = ((), (), s32[]{:S(2)}) async-start(), calls=%async_computation.5 | async-start | bytes 2367488 | tf_op jit(solution)/shard_map/all_gather | solution.py:29
  8.4 5.7 %copy-start.7 = (f32[1,8,64]{2,1,0:T(8,128)}, f32[1,8,64]{2,1,0:T(8,128)S(1)}, u32[]{:S(2)}) copy-start(f32[1,8,64]{2,1,0:T(8,128)S(1)} %reduce_window_sum.28) | copy-start | bytes 6148
  11.3 2.8 copy-start.9
  14.1 57.6 %copy-start.1 = (bf16[256,256]{1,0:T(8,128)(2,1)S(1)}, bf16[256,256]{1,0:T(8,128)(2,1)}, u32[]{:S(2)}) copy-start(bf16[256,256]{1,0:T(8,128)(2,1)} %param.24) | copy-start | bytes 393220
  52.1 0.5 copy-start.15
  52.1 0.5 copy-start.17
  68.2 177.3 %all-gather.7.cloned.1.call-start = ((), (), s32[]{:S(2)}) async-start(), calls=%async_computation.4 | async-start | bytes 8912896 | tf_op jit(solution)/shard_map/all_gather | solution.py:237
  75.7 49.9 %copy-start.8 = (f32[1,8,64]{2,1,0:T(8,128)S(1)}, f32[1,8,64]{2,1,0:T(8,128)}, u32[]{:S(2)}) copy-start(f32[1,8,64]{2,1,0:T(8,128)} %copy-done.7) | copy-start | bytes 6148
  75.7 49.9 %copy-start.10 = (f32[8,64]{1,0:T(8,128)S(1)}, f32[8,64]{1,0:T(8,128)}, u32[]{:S(2)}) copy-start(f32[8,64]{1,0:T(8,128)} %copy-done.9) | copy-start | bytes 6148
  75.7 106.8 %copy-start.16 = (f32[8,1]{0,1:T(1,128)S(1)}, f32[8,1]{0,1:T(1,128)}, u32[]{:S(2)}) copy-start(f32[8,1]{0,1:T(1,128)} %copy-done.15) | copy-start | bytes 100
  75.8 106.8 %copy-start.18 = (f32[8,1]{0,1:T(1,128)S(1)}, f32[8,1]{0,1:T(1,128)}, u32[]{:S(2)}) copy-start(f32[8,1]{0,1:T(1,128)} %copy-done.17) | copy-start | bytes 100
  149.8 100.9 %copy-start.4 = (bf16[1,64,4096]{2,1,0:T(8,128)(2,1)S(1)}, bf16[1,64,4096]{2,1,0:T(8,128)(2,1)}, u32[]{:S(2)}) copy-start(bf16[1,64,4096]{2,1,0:T(8,128)(2,1)} %param.27) | copy-start | bytes 1572868
  245.5 5.8 %copy-start.2 = (bf16[1024,4096]{1,0:T(8,128)(2,1)S(1)}, bf16[1024,4096]{1,0:T(8,128)(2,1)}, u32[]{:S(2)}) copy-start(bf16[1024,4096]{1,0:T(8,128)(2,1)} %all-gather.7.cloned.1.call-done) | copy-start | bytes 25165828
  251.3 2.7 copy-start.20
  258.3 4.9 %copy-start.12 = (f32[8,1,128]{2,1,0:T(1,128)S(1)}, f32[8,1,128]{2,1,0:T(1,128)}, u32[]{:S(2)}) copy-start(f32[8,1,128]{2,1,0:T(1,128)} %get-tuple-element.83) | copy-start | bytes 12292
  258.3 5.0 %copy-start.22 = (bf16[512,128]{1,0:T(8,128)(2,1)S(1)}, bf16[512,128]{1,0:T(8,128)(2,1)}, u32[]{:S(2)}) copy-start(bf16[512,128]{1,0:T(8,128)(2,1)} %param.16) | copy-start | bytes 393220
  258.3 5.3 %copy-start.5 = (bf16[512,128]{1,0:T(8,128)(2,1)S(1)}, bf16[512,128]{1,0:T(8,128)(2,1)}, u32[]{:S(2)}) copy-start(bf16[512,128]{1,0:T(8,128)(2,1)} %param.17) | copy-start | bytes 393220
  258.3 31.3 %all-to-all-start.2 = ((bf16[16,1024,64]{1,2,0:T(8,128)(2,1)}), bf16[16,1024,64]{1,2,0:T(8,128)(2,1)}, u32[]{:S(2)}, u32[]{:S(2)}) async-start(bf16[16,1024,64]{1,2,0:T(8,128)(2,1)} %broadcast_in_dim.75), calls=%async_computation.2 | async-start | bytes 4194304 | tf_op jit(solution)/shard_map/all_to_all | solution.py:61
  263.1 2.8 copy-start.3
  263.2 3.0 copy-start.19
  265.9 1.2 copy-start.6
  265.9 1.2 copy-start.14
  292.1 7.5 %copy-start.21 = (bf16[1,1024,256]{2,1,0:T(8,128)(2,1)S(1)}, bf16[1,1024,256]{2,1,0:T(8,128)(2,1)}, u32[]{:S(2)}) copy-start(bf16[1,1024,256]{2,1,0:T(8,128)(2,1)} %param.29) | copy-start | bytes 1572868
  292.1 66.5 %all-to-all-start = ((bf16[16,512,256]{1,2,0:T(8,128)(2,1)}), bf16[16,512,256]{1,2,0:T(8,128)(2,1)}, u32[]{:S(2)}, u32[]{:S(2)}) async-start(bf16[16,512,256]{1,2,0:T(8,128)(2,1)} %stack.2), calls=%async_computation | async-start | bytes 8388608 | tf_op jit(solution)/shard_map/all_to_all | solution.py:236
  299.5 74.6 %copy-start.11 = (s32[256,2]{0,1:T(2,128)S(1)}, s32[256,2]{0,1:T(2,128)}, u32[]{:S(2)}) copy-start(s32[256,2]{0,1:T(2,128)} %param.25) | copy-start | bytes 6148
  299.5 75.2 %copy-start.13 = (f32[256,2]{0,1:T(2,128)S(1)}, f32[256,2]{0,1:T(2,128)}, u32[]{:S(2)}) copy-start(f32[256,2]{0,1:T(2,128)} %param.26) | copy-start | bytes 6148
  358.6 49.0 %all-to-all-start.3 = ((bf16[32,32,256]{2,1,0:T(8,128)(2,1)}), bf16[32,32,256]{2,1,0:T(8,128)(2,1)S(1)}, u32[]{:S(2)}, u32[]{:S(2)}) async-start(bf16[32,32,256]{2,1,0:T(8,128)(2,1)} %bitcast.141), calls=%async_computation.3 | async-start | bytes 1048576 | tf_op jit(solution)/shard_map/all_to_all | solution.py:249
Sparse Core Ops, SparseCore 0:
  68.3 80.3 all-gather.8
  151.7 93.8 all-gather.6
